TPU v7x, 512 devices: a whole 4x4x16 slice. The times are simulated.
512 devices in a mesh: ep: 128 (over z, x, core), tp: 4 (over y).
Axes of the slice: x: 4, y: 4, z: 16, core: 2. Of those that a mesh axis runs over, the one named last changes fastest.
Arguments:
- tokens: bfloat16 [1024, 2048], P('ep'), may hold values from -6 to 6
- norm_gain: float32 [2048], replicated, may hold values from 0.1 to 1.9
- query_weight: bfloat16 [2048, 1024], P('ep', 'tp'), may hold values from -0.125 to 0.125
- key_weight: bfloat16 [2048, 512], P('ep', 'tp'), may hold values from -0.125 to 0.125
- value_weight: bfloat16 [2048, 512], P('ep', 'tp'), may hold values from -0.125 to 0.125
- query_gain: float32 [64], replicated, may hold values from 0.9 to 1.9
- key_gain: float32 [64], replicated, may hold values from 0.9 to 1.9
- lambdas: float32 [8], P('tp'), may hold values from 0.3 to 0.8
- key_cache: bfloat16 [1024, 4, 320, 128], P('ep', 'tp'), may hold values from -5 to 5
- value_cache: bfloat16 [1024, 4, 320, 128], P('ep', 'tp'), may hold values from -6 to 6
- lengths: int32 [1024], P('ep'), may hold values from 1 to 320
- head_gain: float32 [128], replicated, may hold values from 0.1 to 1.9
- out_weight: bfloat16 [1024, 2048], P('tp', 'ep'), may hold values from -0.1875 to 0.1875
- ffn_gain: float32 [2048], replicated, may hold values from 0.1 to 1.9
- dense_gate_weight: bfloat16 [2048, 1024], P('ep', 'tp'), may hold values from -0.125 to 0.125
- dense_up_weight: bfloat16 [2048, 1024], P('ep', 'tp'), may hold values from -0.125 to 0.125
- dense_down_weight: bfloat16 [1024, 2048], P('tp', 'ep'), may hold values from -0.1875 to 0.1875
- branch_gate: float32 [2048], replicated, may hold values from -0.125 to 0.125
- expert_ids: int32 [1024, 2], P('ep'), may hold values from 0 to 15, all different within a row; in each aligned block of 8 rows (0 to 7, 8 to 15, ...) at most 2 rows name the same one
- expert_probs: float32 [1024, 2], P('ep'), may hold values from 0.1 to 0.9
- expert_gate: bfloat16 [128, 2048, 704], P('ep', None, 'tp'), may hold values from -0.125 to 0.125
- expert_up: bfloat16 [128, 2048, 704], P('ep', None, 'tp'), may hold values from -0.125 to 0.125
- expert_down: bfloat16 [128, 704, 2048], P('ep', 'tp'), may hold values from -0.078125 to 0.078125
Outputs:
- mixed: bfloat16 [1024, 2048], P('ep', 'tp')
Inputs may be any that keep to these rules, and one draw needn't show every extreme that they name: `expert_ids`: each row names 2 different experts. Within each aligned block of 8 rows (the sequences of one index of ep) no expert is named more than 2 times, and in every draw some block names some expert exactly 2 times.
All inputs are finite; a program needn't handle non-finite values.
Results may differ from a plain program's by a relative error of at most 0.014.
Values may be sent and summed in bfloat16 or wider, within the bound.
No kernel may reach another device: no remote copies, remote signals or barrier semaphores. Data moves between devices by JAX's collectives and lax.ppermute only.
A program may use at most 64 MiB of HBM per device.

v0:
```python
import jax
import jax.numpy as jnp
from jax import lax
from jax.sharding import PartitionSpec as P

SUB = 64
VD = 128
EXPERTS = 16
TOP = 2
CAP = 2
epsilon = 1e-06


def rms_scale(values, scaling):
    return values * lax.rsqrt(jnp.mean(values * values, axis=-1, keepdims=True) + epsilon) * scaling


def project_rows(normed, weights):
    stacked = jnp.concatenate(weights, axis=1)
    spread = lax.all_to_all(normed, "ep", split_axis=1, concat_axis=0, tiled=True)
    return lax.psum_scatter(
        jnp.dot(spread, stacked, preferred_element_type=jnp.float32),
        "ep",
        scatter_dimension=0,
        tiled=True,
    )


def project_back(operand, weight):
    products = jnp.dot(
        lax.all_gather(operand, "ep", axis=0, tiled=True),
        weight,
        preferred_element_type=jnp.float32,
    ).astype(jnp.bfloat16)
    partial_value = lax.all_to_all(products, "ep", split_axis=0, concat_axis=1, tiled=True)
    return lax.psum(
        lax.optimization_barrier(partial_value).astype(jnp.float32).astype(jnp.bfloat16), "tp"
    ).astype(jnp.float32)


def attend(packed, key_cache, value_cache, lengths, query_gain, key_gain, lambdas, head_gain):
    seq_here = packed.shape[0]
    kv_here = key_cache.shape[1]
    cache_len = key_cache.shape[2]
    heads_here = lambdas.shape[0]
    per_group = heads_here // kv_here
    query_end = heads_here * 2 * SUB
    key_end = query_end + kv_here * 2 * SUB
    mixed = lax.optimization_barrier(packed.astype(jnp.bfloat16))
    query_parts = rms_scale(
        mixed[:, :query_end].astype(jnp.float32).reshape(seq_here, kv_here, per_group, 2, SUB),
        query_gain,
    ).astype(jnp.bfloat16)
    key_parts = rms_scale(
        mixed[:, query_end:key_end].astype(jnp.float32).reshape(seq_here, kv_here, 2, SUB), key_gain
    ).astype(jnp.bfloat16)
    new_values = mixed[:, key_end:].reshape(seq_here, kv_here, VD)
    cached = rms_scale(
        key_cache.astype(jnp.float32).reshape(seq_here, kv_here, cache_len, 2, SUB), key_gain
    ).astype(jnp.bfloat16)
    score_scale = SUB ** (-0.5)
    scores = (
        jnp.einsum("sgqcd,sgjcd->sgqcj", query_parts, cached, preferred_element_type=jnp.float32)
        * score_scale
    )
    own_score = (
        jnp.einsum("sgqcd,sgcd->sgqc", query_parts, key_parts, preferred_element_type=jnp.float32)
        * score_scale
    )
    live_mask = lax.broadcasted_iota(jnp.int32, (seq_here, cache_len), 1) < lengths[:, None]
    exponent = jnp.where(live_mask[:, None, None, None, :], jnp.exp(scores), 0.0)
    own_exponent = jnp.exp(own_score)
    denominator = jnp.sum(exponent, axis=4) + own_exponent
    shares = exponent / denominator[..., None]
    own_shares = own_exponent / denominator
    lam_heads = lambdas.reshape(1, kv_here, per_group)
    mixing = (shares[:, :, :, 0] - lam_heads[..., None] * shares[:, :, :, 1]).astype(jnp.bfloat16)
    own_mixing = lax.optimization_barrier(
        (own_shares[:, :, :, 0] - lam_heads * own_shares[:, :, :, 1]).astype(jnp.bfloat16)
    )
    head_out = jnp.einsum(
        "sgqj,sgje->sgqe", mixing, value_cache, preferred_element_type=jnp.float32
    )
    head_out = (
        head_out
        + own_mixing.astype(jnp.float32)[..., None] * new_values.astype(jnp.float32)[:, :, None, :]
    )
    return rms_scale(head_out, head_gain).astype(jnp.bfloat16).reshape(seq_here, heads_here * VD)


def route_tables(expert_ids, expert_probs):
    seq_here = expert_ids.shape[0]
    paired = expert_ids.reshape(-1)
    total_pairs = paired.shape[0]
    onehot = (paired[:, None] == lax.broadcasted_iota(jnp.int32, (total_pairs, EXPERTS), 1)).astype(
        jnp.float32
    )
    earlier = (
        lax.broadcasted_iota(jnp.int32, (total_pairs, total_pairs), 1)
        < lax.broadcasted_iota(jnp.int32, (total_pairs, total_pairs), 0)
    ).astype(jnp.float32)
    before = jnp.dot(earlier, onehot, precision=lax.Precision.HIGHEST)
    slot_ranks = jnp.sum(before * onehot, axis=1).astype(jnp.int32)
    slot_codes = (paired * CAP + slot_ranks).reshape(seq_here, TOP)
    slots_iota = lax.broadcasted_iota(jnp.int32, (seq_here, TOP, EXPERTS * CAP), 2)
    picked = (slot_codes[:, :, None] == slots_iota).astype(jnp.float32)
    select = jnp.sum(picked, axis=1)
    combine_weights = jnp.sum(picked * expert_probs[:, :, None], axis=1)
    return (select, combine_weights)


def mixture(ffn_input, expert_ids, expert_probs, expert_gate, expert_up, expert_down):
    here_count = expert_gate.shape[0]
    ep_count = lax.axis_size("ep")
    tp_count = lax.axis_size("tp")
    slot_count = ep_count * here_count
    rep_count = slot_count // EXPERTS
    model_width = ffn_input.shape[1]
    feature_share = model_width // tp_count
    select, combine_weights = route_tables(expert_ids, expert_probs)
    sent_width = ffn_input.shape[1]
    chosen = jnp.einsum(
        "sk,sd->kd", select.astype(jnp.bfloat16), ffn_input, preferred_element_type=jnp.float32
    ).astype(jnp.bfloat16)
    outgoing = jnp.broadcast_to(
        chosen.reshape(1, EXPERTS, CAP, sent_width), (rep_count, EXPERTS, CAP, sent_width)
    ).reshape(slot_count, CAP, sent_width)
    incoming = lax.all_to_all(outgoing, "ep", split_axis=0, concat_axis=0, tiled=True)
    grouped = incoming.reshape(ep_count, here_count, incoming.shape[1], model_width)
    gate_val = jnp.einsum(
        "ihcd,hdf->ihcf", grouped, expert_gate, preferred_element_type=jnp.float32
    )
    up_val = jnp.einsum("ihcd,hdf->ihcf", grouped, expert_up, preferred_element_type=jnp.float32)
    hidden = (jax.nn.silu(gate_val) * up_val).astype(jnp.bfloat16)
    partial_value = jnp.einsum(
        "ihcf,hfd->ihcd", hidden, expert_down, preferred_element_type=jnp.float32
    ).astype(jnp.bfloat16)
    summed = lax.all_to_all(partial_value, "tp", split_axis=3, concat_axis=0, tiled=True)
    block_out = jnp.sum(
        summed.reshape(tp_count, ep_count, here_count, CAP, feature_share).astype(jnp.float32),
        axis=0,
    ).astype(jnp.bfloat16)
    returned = lax.all_to_all(block_out, "ep", split_axis=0, concat_axis=0, tiled=True)
    expert_out = jnp.sum(
        returned.reshape(rep_count, EXPERTS * CAP, feature_share).astype(jnp.float32), axis=0
    )
    return jnp.dot(combine_weights, expert_out, precision=lax.Precision.HIGHEST)


def own_columns(values, tp_start, share_width):
    return lax.dynamic_slice_in_dim(values, tp_start, share_width, 1)


def shards(
    tokens,
    norm_gain,
    query_weight,
    key_weight,
    value_weight,
    query_gain,
    key_gain,
    lambdas,
    key_cache,
    value_cache,
    lengths,
    head_gain,
    out_weight,
    ffn_gain,
    dense_gate_weight,
    dense_up_weight,
    dense_down_weight,
    branch_gate,
    expert_ids,
    expert_probs,
    expert_gate,
    expert_up,
    expert_down,
):
    residual = tokens.astype(jnp.float32)
    normed = rms_scale(residual, norm_gain).astype(jnp.bfloat16)
    packed = project_rows(normed, (query_weight, key_weight, value_weight))
    head_out = attend(
        packed, key_cache, value_cache, lengths, query_gain, key_gain, lambdas, head_gain
    )
    attended = project_back(head_out, out_weight)
    middle = lax.optimization_barrier((residual + attended).astype(jnp.bfloat16))
    middle_f32 = middle.astype(jnp.float32)
    ffn_input = lax.optimization_barrier(rms_scale(middle_f32, ffn_gain).astype(jnp.bfloat16))
    dense_both = project_rows(ffn_input, (dense_gate_weight, dense_up_weight))
    half_width = dense_both.shape[1] // 2
    hidden = (jax.nn.silu(dense_both[:, :half_width]) * dense_both[:, half_width:]).astype(
        jnp.bfloat16
    )
    dense = project_back(hidden, dense_down_weight)
    branch_weight = jax.nn.sigmoid(
        jnp.sum(ffn_input.astype(jnp.float32) * branch_gate, axis=1, keepdims=True)
    )
    routed = mixture(ffn_input, expert_ids, expert_probs, expert_gate, expert_up, expert_down)
    share_width = routed.shape[1]
    tp_start = lax.axis_index("tp") * share_width
    combined = (
        own_columns(middle_f32, tp_start, share_width)
        + own_columns(branch_weight * dense, tp_start, share_width)
        + routed
    )
    return combined.astype(jnp.bfloat16)


def solution(mesh):
    return jax.shard_map(
        shards,
        mesh=mesh,
        in_specs=(
            P("ep", None),
            P(),
            P("ep", "tp"),
            P("ep", "tp"),
            P("ep", "tp"),
            P(),
            P(),
            P("tp"),
            P("ep", "tp", None, None),
            P("ep", "tp", None, None),
            P("ep"),
            P(),
            P("tp", "ep"),
            P(),
            P("ep", "tp"),
            P("ep", "tp"),
            P("tp", "ep"),
            P(),
            P("ep", None),
            P("ep", None),
            P("ep", None, "tp"),
            P("ep", None, "tp"),
            P("ep", "tp", None),
        ),
        out_specs=P("ep", "tp"),
        check_vma=False,
    )
```

profile of v0, /device:TPU:33, one launch (start us, length us, event | category | flops | bytes accessed | tf_op | source)
XLA Modules:
  0.0 908.0 jit_solution(11844619829971463060)
XLA Ops:
  6.5 1.0 fusion.32
  7.5 0.8 fusion.34
  8.8 41.7 %all_to_all.98 = bf16[8,128,16]{2,0,1:T(8,128)(2,1)S(1)} all-to-all(bf16[8,128,16]{2,0,1:T(8,128)(2,1)S(1)} %copy.97), channel_id=1, replica_groups=mesh['ep'=128,'tp'=4] {'ep'}, dimensions={1} | all-to-all | bytes 65536 | tf_op jit(solution)/shard_map/all_to_all | solution.py:20
  50.4 2.5 fusion.24
  52.9 1.1 copy-done.2
  55.5 239.6 %reduce-scatter.3.cloned.1.call-done = f32[8,512]{1,0:T(8,128)} async-done(((f32[1024,512]{1,0:T(8,128)}), f32[8,512]{1,0:T(8,128)}) %reduce-scatter.3.cloned.1.call-update) | async-done | bytes 16400 | tf_op jit(solution)/shard_map/reduce_scatter | solution.py:21
  298.4 93.9 %all_gather.6 = bf16[1024,256]{1,0:T(8,128)(2,1)S(1)} all-gather(bf16[8,256]{1,0:T(8,128)(2,1)S(1)} %bitcast.148), channel_id=1, replica_groups=mesh['ep'=128,'tp'=4] {'ep'}, dimensions={0}, use_global_device_ids=true | all-gather | bytes 528384 | tf_op jit(solution)/shard_map/all_gather | solution.py:31
  392.6 0.9 copy.106
  393.4 12.8 %all-to-all-start.1 = ((bf16[128,8,16]{2,1,0:T(8,128)(2,1)}), bf16[128,8,16]{2,1,0:T(8,128)(2,1)S(1)}, u32[]{:S(2)}, u32[]{:S(2)}) async-start(bf16[128,8,16]{2,1,0:T(8,128)(2,1)} %bitcast.18), calls=%async_computation.2 | async-start | bytes 524288 | tf_op jit(solution)/shard_map/all_to_all | solution.py:35
  406.4 22.4 %all-to-all-done.1 = bf16[128,8,16]{2,1,0:T(8,128)(2,1)S(1)} async-done(((bf16[128,8,16]{2,1,0:T(8,128)(2,1)}), bf16[128,8,16]{2,1,0:T(8,128)(2,1)S(1)}, u32[]{:S(2)}, u32[]{:S(2)}) %all-to-all-start.1) | async-done | bytes 32800 | tf_op jit(solution)/shard_map/all_to_all | solution.py:35
  429.2 13.3 %psum.14 = bf16[8,2048]{1,0:T(8,128)(2,1)S(1)} all-reduce(bf16[8,2048]{1,0:T(8,128)(2,1)S(1)} %all_to_all.78), channel_id=1, replica_groups=mesh['ep'=128,'tp'=4] {'tp'}, use_global_device_ids=true, to_apply=%region_7.8 | all-reduce | flops 16384 | bytes 65536 | tf_op jit(solution)/shard_map/psum | solution.py:36
  443.4 0.9 copy.108
  444.3 9.9 %all-to-all-start.2 = ((bf16[8,128,16]{2,0,1:T(8,128)(2,1)}), bf16[8,128,16]{2,0,1:T(8,128)(2,1)S(1)}, u32[]{:S(2)}, u32[]{:S(2)}) async-start(bf16[8,128,16]{2,0,1:T(8,128)(2,1)} %copy.108), calls=%async_computation.3 | async-start | bytes 524288 | tf_op jit(solution)/shard_map/all_to_all | solution.py:20
  454.6 22.2 %all-to-all-done.2 = bf16[8,128,16]{2,0,1:T(8,128)(2,1)S(1)} async-done(((bf16[8,128,16]{2,0,1:T(8,128)(2,1)}), bf16[8,128,16]{2,0,1:T(8,128)(2,1)S(1)}, u32[]{:S(2)}, u32[]{:S(2)}) %all-to-all-start.2) | async-done | bytes 32800 | tf_op jit(solution)/shard_map/all_to_all | solution.py:20
  476.8 1.7 broadcast_in_dim.19
  478.5 6.2 all-to-all-start.4
  484.8 1.7 fusion.22
  486.5 53.7 %all-to-all-done.4 = bf16[128,2,2048]{2,1,0:T(2,128)(2,1)S(1)} async-done(((bf16[128,2,2048]{2,1,0:T(2,128)(2,1)}), bf16[128,2,2048]{2,1,0:T(2,128)(2,1)S(1)}, u32[]{:S(2)}, u32[]{:S(2)}) %all-to-all-start.4) | async-done | bytes 1048608 | tf_op jit(solution)/shard_map/all_to_all | solution.py:128
  540.3 1.5 convolution_bitcast_fusion.1
  541.8 2.4 fusion
  544.1 2.0 copy.116
  546.2 3.6 all-to-all-start.5
  549.8 190.6 %reduce-scatter.5.cloned.1.call-done = f32[8,512]{1,0:T(8,128)} async-done(((f32[1024,512]{1,0:T(8,128)}), f32[8,512]{1,0:T(8,128)}) %reduce-scatter.5.cloned.1.call-update) | async-done | bytes 16400 | tf_op jit(solution)/shard_map/reduce_scatter | solution.py:21
  741.2 93.9 %all_gather.7 = bf16[1024,256]{1,0:T(8,128)(2,1)S(1)} all-gather(bf16[8,256]{1,0:T(8,128)(2,1)S(1)} %fusion.50), channel_id=1, replica_groups=mesh['ep'=128,'tp'=4] {'ep'}, dimensions={0}, use_global_device_ids=true | all-gather | bytes 528384 | tf_op jit(solution)/shard_map/all_gather | solution.py:31
  835.3 0.9 copy.109
  836.1 12.8 %all-to-all-start.3 = ((bf16[128,8,16]{2,1,0:T(8,128)(2,1)}), bf16[128,8,16]{2,1,0:T(8,128)(2,1)S(1)}, u32[]{:S(2)}, u32[]{:S(2)}) async-start(bf16[128,8,16]{2,1,0:T(8,128)(2,1)} %bitcast.22), calls=%async_computation.5 | async-start | bytes 524288 | tf_op jit(solution)/shard_map/all_to_all | solution.py:35
  849.0 1.6 reduce_sum.136
  850.7 1.0 copy.118
  851.7 19.8 %all-to-all-done.3 = bf16[128,8,16]{2,1,0:T(8,128)(2,1)S(1)} async-done(((bf16[128,8,16]{2,1,0:T(8,128)(2,1)}), bf16[128,8,16]{2,1,0:T(8,128)(2,1)S(1)}, u32[]{:S(2)}, u32[]{:S(2)}) %all-to-all-start.3) | async-done | bytes 32800 | tf_op jit(solution)/shard_map/all_to_all | solution.py:35
  871.5 6.2 all-to-all-start.6
  878.3 14.5 %psum.15 = bf16[8,2048]{1,0:T(8,128)(2,1)S(1)} all-reduce(bf16[8,2048]{1,0:T(8,128)(2,1)S(1)} %all_to_all.86), channel_id=1, replica_groups=mesh['ep'=128,'tp'=4] {'tp'}, use_global_device_ids=true, to_apply=%region_11.12 | all-reduce | flops 16384 | bytes 65536 | tf_op jit(solution)/shard_map/psum | solution.py:36
  892.8 7.5 all-to-all-done.6
  (120 shorter events, 9.7 us)
Async XLA Ops:
  6.5 535.2 %copy-start = (bf16[1,176,2048]{2,1,0:T(8,128)(2,1)S(1)}, bf16[1,176,2048]{2,1,0:T(8,128)(2,1)}, u32[]{:S(2)}) copy-start(bf16[1,176,2048]{2,1,0:T(8,128)(2,1)} %param.45) | copy-start | bytes 2162692
  6.5 288.6 %reduce-scatter.3.cloned.1.call-start = ((), (), s32[]{:S(2)}) async-start(), calls=%async_computation.9 | async-start | bytes 2113536 | tf_op jit(solution)/shard_map/reduce_scatter | solution.py:21
  52.9 1.1 copy-start.2
  52.9 1.5 copy-start.14
  54.8 0.7 copy-start.17
  54.8 241.8 %copy-start.18 = (f32[64]{0:T(128)S(1)}, f32[64]{0:T(128)}, u32[]{:S(2)}) copy-start(f32[64]{0:T(128)} %param.29) | copy-start | bytes 772
  54.8 241.9 %copy-start.16 = (f32[64]{0:T(128)S(1)}, f32[64]{0:T(128)}, u32[]{:S(2)}) copy-start(f32[64]{0:T(128)} %param.28) | copy-start | bytes 772
  54.9 242.7 %copy-start.20 = (f32[2]{0:T(128)S(1)}, f32[2]{0:T(128)}, u32[]{:S(2)}) copy-start(f32[2]{0:T(128)} %param.30) | copy-start | bytes 28
  55.4 242.5 %copy-start.22 = (bf16[8,1,320,128]{3,2,1,0:T(8,128)(2,1)S(1)}, bf16[8,1,320,128]{3,2,1,0:T(8,128)(2,1)}, u32[]{:S(2)}) copy-start(bf16[8,1,320,128]{3,2,1,0:T(8,128)(2,1)} %param.32) | copy-start | bytes 1966084
  55.4 242.9 %copy-start.19 = (f32[128]{0:T(128)S(1)}, f32[128]{0:T(128)}, u32[]{:S(2)}) copy-start(f32[128]{0:T(128)} %param.34) | copy-start | bytes 1540
  297.0 95.3 %copy-start.8 = (bf16[256,16]{0,1:T(8,128)(2,1)S(1)}, bf16[256,16]{0,1:T(8,128)(2,1)}, u32[]{:S(2)}) copy-start(bf16[256,16]{0,1:T(8,128)(2,1)} %param.35) | copy-start | bytes 24580
  297.5 108.9 %copy-start.15 = (f32[8,2]{0,1:T(2,128)S(1)}, f32[8,2]{0,1:T(2,128)}, u32[]{:S(2)}) copy-start(f32[8,2]{0,1:T(2,128)} %param.42) | copy-start | bytes 196
  298.3 144.2 %copy-start.7 = (bf16[8,2048]{1,0:T(8,128)(2,1)S(1)}, bf16[8,2048]{1,0:T(8,128)(2,1)}, u32[]{:S(2)}) copy-start(bf16[8,2048]{1,0:T(8,128)(2,1)} %param.23) | copy-start | bytes 98308
  298.3 144.8 %copy-start.12 = (f32[2048]{0:T(1024)S(1)}, f32[2048]{0:T(1024)}, u32[]{:S(2)}) copy-start(f32[2048]{0:T(1024)} %param.36) | copy-start | bytes 24580
  393.4 35.4 %all-to-all-start.1 = ((bf16[128,8,16]{2,1,0:T(8,128)(2,1)}), bf16[128,8,16]{2,1,0:T(8,128)(2,1)S(1)}, u32[]{:S(2)}, u32[]{:S(2)}) async-start(bf16[128,8,16]{2,1,0:T(8,128)(2,1)} %bitcast.18), calls=%async_computation.2 | async-start | bytes 524288 | tf_op jit(solution)/shard_map/all_to_all | solution.py:35
  442.5 0.6 copy-start.3
  443.2 35.3 %copy-start.5 = (bf16[8,2048]{1,0:T(8,128)(2,1)}, bf16[8,2048]{1,0:T(8,128)(2,1)S(1)}, u32[]{:S(2)}) copy-start(bf16[8,2048]{1,0:T(8,128)(2,1)S(1)} %multiply_convert_fusion.2) | copy-start | bytes 98308
  444.3 32.5 %all-to-all-start.2 = ((bf16[8,128,16]{2,0,1:T(8,128)(2,1)}), bf16[8,128,16]{2,0,1:T(8,128)(2,1)S(1)}, u32[]{:S(2)}, u32[]{:S(2)}) async-start(bf16[8,128,16]{2,0,1:T(8,128)(2,1)} %copy.108), calls=%async_computation.3 | async-start | bytes 524288 | tf_op jit(solution)/shard_map/all_to_all | solution.py:20
  454.6 30.2 %copy-start.9 = (bf16[16,256]{1,0:T(8,128)(2,1)S(1)}, bf16[16,256]{1,0:T(8,128)(2,1)}, u32[]{:S(2)}) copy-start(bf16[16,256]{1,0:T(8,128)(2,1)} %param.38) | copy-start | bytes 24580
  454.6 30.2 %copy-start.10 = (bf16[16,256]{1,0:T(8,128)(2,1)S(1)}, bf16[16,256]{1,0:T(8,128)(2,1)}, u32[]{:S(2)}) copy-start(bf16[16,256]{1,0:T(8,128)(2,1)} %param.37) | copy-start | bytes 24580
  478.5 61.8 %all-to-all-start.4 = ((bf16[128,2,2048]{2,1,0:T(2,128)(2,1)}), bf16[128,2,2048]{2,1,0:T(2,128)(2,1)S(1)}, u32[]{:S(2)}, u32[]{:S(2)}) async-start(bf16[128,2,2048]{2,1,0:T(2,128)(2,1)} %bitcast.24), calls=%async_computation.6 | async-start | bytes 2097152 | tf_op jit(solution)/shard_map/all_to_all | solution.py:128
  484.7 255.7 %reduce-scatter.5.cloned.1.call-start = ((), (), s32[]{:S(2)}) async-start(), calls=%async_computation.10 | async-start | bytes 2113536 | tf_op jit(solution)/shard_map/reduce_scatter | solution.py:21
  486.5 53.8 %copy-start.21 = (bf16[1,2048,176]{1,2,0:T(8,128)(2,1)S(1)}, bf16[1,2048,176]{1,2,0:T(8,128)(2,1)}, u32[]{:S(2)}) copy-start(bf16[1,2048,176]{1,2,0:T(8,128)(2,1)} %param.43) | copy-start | bytes 2162692
  486.5 55.2 %copy-start.1 = (bf16[1,2048,176]{1,2,0:T(8,128)(2,1)S(1)}, bf16[1,2048,176]{1,2,0:T(8,128)(2,1)}, u32[]{:S(2)}) copy-start(bf16[1,2048,176]{1,2,0:T(8,128)(2,1)} %param.44) | copy-start | bytes 2162692
  546.2 288.9 %copy-start.11 = (bf16[256,16]{0,1:T(8,128)(2,1)S(1)}, bf16[256,16]{0,1:T(8,128)(2,1)}, u32[]{:S(2)}) copy-start(bf16[256,16]{0,1:T(8,128)(2,1)} %param.39) | copy-start | bytes 24580
  546.2 290.0 %all-to-all-start.5 = ((bf16[128,1,2,2048]{0,2,1,3:T(2,128)(2,1)}), bf16[128,1,2,2048]{0,2,1,3:T(2,128)(2,1)S(1)}, u32[]{:S(2)}, u32[]{:S(2)}) async-start(bf16[128,1,2,2048]{0,2,1,3:T(2,128)(2,1)} %copy.116), calls=%async_computation.7 | async-start | bytes 2097152 | tf_op jit(solution)/shard_map/all_to_all | solution.py:138
  836.1 35.4 %all-to-all-start.3 = ((bf16[128,8,16]{2,1,0:T(8,128)(2,1)}), bf16[128,8,16]{2,1,0:T(8,128)(2,1)S(1)}, u32[]{:S(2)}, u32[]{:S(2)}) async-start(bf16[128,8,16]{2,1,0:T(8,128)(2,1)} %bitcast.22), calls=%async_computation.5 | async-start | bytes 524288 | tf_op jit(solution)/shard_map/all_to_all | solution.py:35
  849.0 28.8 %copy-start.4 = (bf16[8,2048]{1,0:T(8,128)(2,1)S(1)}, bf16[8,2048]{1,0:T(8,128)(2,1)}, u32[]{:S(2)}) copy-start(bf16[8,2048]{1,0:T(8,128)(2,1)} %copy-done.3) | copy-start | bytes 98308
  849.0 28.8 %copy-start.6 = (bf16[8,2048]{1,0:T(8,128)(2,1)S(1)}, bf16[8,2048]{1,0:T(8,128)(2,1)}, u32[]{:S(2)}) copy-start(bf16[8,2048]{1,0:T(8,128)(2,1)} %copy-done.5) | copy-start | bytes 98308
  849.0 28.8 %copy-start.13 = (f32[2048]{0:T(1024)S(1)}, f32[2048]{0:T(1024)}, u32[]{:S(2)}) copy-start(f32[2048]{0:T(1024)} %param.40) | copy-start | bytes 24580
  871.5 28.8 %all-to-all-start.6 = ((bf16[128,1,2,512]{3,2,1,0:T(2,128)(2,1)}), bf16[128,1,2,512]{3,2,1,0:T(2,128)(2,1)S(1)}, u32[]{:S(2)}, u32[]{:S(2)}) async-start(bf16[128,1,2,512]{3,2,1,0:T(2,128)(2,1)} %copy.118), calls=%async_computation.8 | async-start | bytes 524288 | tf_op jit(solution)/shard_map/all_to_all | solution.py:143
Sparse Core Ops, SparseCore 0:
  53.0 242.0 reduce-scatter.2
  490.1 250.2 reduce-scatter.4
where the time goes:
time: 909 us; the launch traced here: 908 us
  waiting for transfers between devices  556 us (61%)
  blocking collectives  257 us (28%)
  starting transfers between devices  51.6 us (6%)
  between operations  13.8 us (2%)
  local copies, waits for them, and re-layouts  12.5 us (1%)
  matrix products  10.6 us (1%)
    reduce_scatter x2, waiting for transfers between devices, project_rows(): lax.psum_scatter(jnp.dot(spread, stacked, preferred_element_type=jnp.floa...  430 us
    all_gather x2, blocking collectives, project_back(): lax.all_gather(operand, 'ep', axis=0, tiled=True)  188 us
    all_to_all x1, waiting for transfers between devices, mixture(): lax.all_to_all(outgoing, 'ep', split_axis=0, concat_axis=0, tiled=True)  53.7 us
    all_to_all x2, waiting for transfers between devices, project_back(): lax.all_to_all(products, 'ep', split_axis=0, concat_axis=1, tiled=True)  42.2 us
    all_to_all x1, blocking collectives, project_rows(): lax.all_to_all(normed, 'ep', split_axis=1, concat_axis=0, tiled=True)  41.7 us
    psum x2, blocking collectives, project_back(): lax.psum(lax.optimization_barrier(partial_value).astype(jnp.float32).asty...  27.8 us
    all_to_all x2, starting transfers between devices, project_back(): lax.all_to_all(products, 'ep', split_axis=0, concat_axis=1, tiled=True)  25.6 us
    all_to_all x1, waiting for transfers between devices, project_rows(): lax.all_to_all(normed, 'ep', split_axis=1, concat_axis=0, tiled=True)  22.2 us
  transfers between devices with their start and end apart: 8, of which 7 were waited for; matrix products, arithmetic and copies ran while one was open for 2% of the time, Pallas kernels for 0%

commit v1 on v0

--- a/solution.py
+++ b/solution.py
@@ -28,7 +28,9 @@
 
 def project_back(operand, weight):
     products = jnp.dot(
-        lax.all_gather(operand, "ep", axis=0, tiled=True),
+        jnp.concatenate(
+            lax.all_to_all(jnp.stack([operand] * lax.axis_size("ep")), "ep", 0, 0), axis=0
+        ),
         weight,
         preferred_element_type=jnp.float32,
     ).astype(jnp.bfloat16)

time: 909 us -> 845 us (0.930)
  blocking collectives: 257 us -> 67.8 us
  waiting for transfers between devices: 556 us -> 642 us
  starting transfers between devices: 51.6 us -> 89.4 us
    all_gather x2 -> x0, blocking collectives: 188 us -> none  [project_back(): lax.all_gather(operand, 'ep', axis=0, tiled=True)]
    reduce_scatter x2, waiting for transfers between devices: 430 us -> 494 us  [project_rows(): lax.psum_scatter(jnp.dot(spread, stacked, preferred_element_type=jnp.floa...]
    all_to_all x0 -> x2, waiting for transfers between devices: none -> 60.9 us  [project_back(): lax.all_to_all(jnp.stack([operand] * lax.axis_size('ep')), 'ep', 0, 0)]
    all_to_all x1, waiting for transfers between devices: 53.7 us -> 0.01 us  [mixture(): lax.all_to_all(outgoing, 'ep', split_axis=0, concat_axis=0, tiled=True)]
    all_to_all x0 -> x2, starting transfers between devices: none -> 50.4 us  [project_back(): lax.all_to_all(jnp.stack([operand] * lax.axis_size('ep')), 'ep', 0, 0)]
    all_to_all x1, waiting for transfers between devices: 0.01 us -> 14 us  [mixture(): lax.all_to_all(partial_value, 'tp', split_axis=3, concat_axis=0, tiled=True)]
    all_to_all x2, starting transfers between devices: 25.6 us -> 12.6 us  [project_back(): lax.all_to_all(products, 'ep', split_axis=0, concat_axis=1, tiled=True)]
  transfers between devices with their start and end apart: 8 -> 10, of which waited for: 7 -> 9; matrix products, arithmetic and copies ran while one was open for 2% -> 2% of each run, Pallas kernels for 0% -> 0%
where the time goes in v1:
time: 845 us; the launch traced here: 844 us
  waiting for transfers between devices  642 us (76%)
  starting transfers between devices  89.4 us (11%)
  blocking collectives  67.8 us (8%)
  between operations  13.8 us (2%)
  local copies, waits for them, and re-layouts  13.7 us (2%)
  matrix products  10.8 us (1%)
    reduce_scatter x2, waiting for transfers between devices, project_rows(): lax.psum_scatter(jnp.dot(spread, stacked, preferred_element_type=jnp.floa...  494 us
    all_to_all x2, waiting for transfers between devices, project_back(): lax.all_to_all(jnp.stack([operand] * lax.axis_size('ep')), 'ep', 0, 0)  60.9 us
    all_to_all x2, starting transfers between devices, project_back(): lax.all_to_all(jnp.stack([operand] * lax.axis_size('ep')), 'ep', 0, 0)  50.4 us
    all_to_all x2, waiting for transfers between devices, project_back(): lax.all_to_all(products, 'ep', split_axis=0, concat_axis=1, tiled=True)  42.4 us
    all_to_all x1, blocking collectives, project_rows(): lax.all_to_all(normed, 'ep', split_axis=1, concat_axis=0, tiled=True)  41.7 us
    psum x2, blocking collectives, project_back(): lax.psum(lax.optimization_barrier(partial_value).astype(jnp.float32).asty...  26.2 us
    all_to_all x1, waiting for transfers between devices, project_rows(): lax.all_to_all(normed, 'ep', split_axis=1, concat_axis=0, tiled=True)  22.2 us
  transfers between devices with their start and end apart: 10, of which 9 were waited for; matrix products, arithmetic and copies ran while one was open for 2% of the time, Pallas kernels for 0%

profile of v1, /device:TPU:33, one launch (start us, length us, event | category | flops | bytes accessed | tf_op | source)
XLA Modules:
  0.0 844.3 jit_solution(6923498952099144837)
XLA Ops:
  6.5 1.0 fusion.34
  8.8 41.7 %all_to_all.108 = bf16[8,128,16]{2,0,1:T(8,128)(2,1)S(1)} all-to-all(bf16[8,128,16]{2,0,1:T(8,128)(2,1)S(1)} %copy.97), channel_id=1, replica_groups=mesh['ep'=128,'tp'=4] {'ep'}, dimensions={1} | all-to-all | bytes 65536 | tf_op jit(solution)/shard_map/all_to_all | solution.py:20
  50.4 2.5 fusion.26
  52.9 1.1 copy-done.1
  55.1 240.0 %reduce-scatter.3.cloned.1.call-done = f32[8,512]{1,0:T(8,128)} async-done(((f32[1024,512]{1,0:T(8,128)}), f32[8,512]{1,0:T(8,128)}) %reduce-scatter.3.cloned.1.call-update) | async-done | bytes 16400 | tf_op jit(solution)/shard_map/reduce_scatter | solution.py:21
  299.2 25.3 %all-to-all-start.1 = ((bf16[128,8,256]{2,1,0:T(8,128)(2,1)}), bf16[128,8,256]{2,1,0:T(8,128)(2,1)S(1)}, u32[]{:S(2)}, u32[]{:S(2)}) async-start(bf16[128,8,256]{2,1,0:T(8,128)(2,1)} %stack.4), calls=%async_computation.2 | async-start | bytes 1048576 | tf_op jit(solution)/shard_map/all_to_all | solution.py:32
  324.9 33.3 %all-to-all-done.1 = bf16[128,8,256]{2,1,0:T(8,128)(2,1)S(1)} async-done(((bf16[128,8,256]{2,1,0:T(8,128)(2,1)}), bf16[128,8,256]{2,1,0:T(8,128)(2,1)S(1)}, u32[]{:S(2)}, u32[]{:S(2)}) %all-to-all-start.1) | async-done | bytes 524320 | tf_op jit(solution)/shard_map/all_to_all | solution.py:32
  359.3 6.2 all-to-all-start.2
  365.7 22.4 %all-to-all-done.2 = bf16[128,8,16]{2,1,0:T(8,128)(2,1)S(1)} async-done(((bf16[128,8,16]{2,1,0:T(8,128)(2,1)}), bf16[128,8,16]{2,1,0:T(8,128)(2,1)S(1)}, u32[]{:S(2)}, u32[]{:S(2)}) %all-to-all-start.2) | async-done | bytes 32800 | tf_op jit(solution)/shard_map/all_to_all | solution.py:37
  388.5 13.3 %psum.14 = bf16[8,2048]{1,0:T(8,128)(2,1)S(1)} all-reduce(bf16[8,2048]{1,0:T(8,128)(2,1)S(1)} %all_to_all.85), channel_id=1, replica_groups=mesh['ep'=128,'tp'=4] {'tp'}, use_global_device_ids=true, to_apply=%region_7.8 | all-reduce | flops 16384 | bytes 65536 | tf_op jit(solution)/shard_map/psum | solution.py:38
  402.3 0.9 copy.108
  403.1 9.9 %all-to-all-start.3 = ((bf16[8,128,16]{2,0,1:T(8,128)(2,1)}), bf16[8,128,16]{2,0,1:T(8,128)(2,1)S(1)}, u32[]{:S(2)}, u32[]{:S(2)}) async-start(bf16[8,128,16]{2,0,1:T(8,128)(2,1)} %copy.108), calls=%async_computation.4 | async-start | bytes 524288 | tf_op jit(solution)/shard_map/all_to_all | solution.py:20
  413.4 22.2 %all-to-all-done.3 = bf16[8,128,16]{2,0,1:T(8,128)(2,1)S(1)} async-done(((bf16[8,128,16]{2,0,1:T(8,128)(2,1)}), bf16[8,128,16]{2,0,1:T(8,128)(2,1)S(1)}, u32[]{:S(2)}, u32[]{:S(2)}) %all-to-all-start.3) | async-done | bytes 32800 | tf_op jit(solution)/shard_map/all_to_all | solution.py:20
  435.6 1.7 broadcast_in_dim.19
  437.3 6.2 all-to-all-start.6
  443.6 1.7 fusion.24
  445.4 253.9 %reduce-scatter.5.cloned.1.call-done = f32[8,512]{1,0:T(8,128)} async-done(((f32[1024,512]{1,0:T(8,128)}), f32[8,512]{1,0:T(8,128)}) %reduce-scatter.5.cloned.1.call-update) | async-done | bytes 16400 | tf_op jit(solution)/shard_map/reduce_scatter | solution.py:21
  700.9 25.1 %all-to-all-start.4 = ((bf16[128,8,256]{2,1,0:T(8,128)(2,1)}), bf16[128,8,256]{2,1,0:T(8,128)(2,1)S(1)}, u32[]{:S(2)}, u32[]{:S(2)}) async-start(bf16[128,8,256]{2,1,0:T(8,128)(2,1)} %stack.5), calls=%async_computation.6 | async-start | bytes 1048576 | tf_op jit(solution)/shard_map/all_to_all | solution.py:32
  726.0 1.5 convolution_bitcast_fusion.1
  727.5 2.6 fusion
  730.1 2.0 copy.116
  732.1 27.6 %all-to-all-done.4 = bf16[128,8,256]{2,1,0:T(8,128)(2,1)S(1)} async-done(((bf16[128,8,256]{2,1,0:T(8,128)(2,1)}), bf16[128,8,256]{2,1,0:T(8,128)(2,1)S(1)}, u32[]{:S(2)}, u32[]{:S(2)}) %all-to-all-start.4) | async-done | bytes 524320 | tf_op jit(solution)/shard_map/all_to_all | solution.py:32
  759.7 4.0 all-to-all-start.7
  764.0 0.9 copy.109
  764.9 14.0 %all-to-all-done.7 = bf16[128,1,2,2048]{0,2,1,3:T(2,128)(2,1)S(1)} async-done(((bf16[128,1,2,2048]{0,2,1,3:T(2,128)(2,1)}), bf16[128,1,2,2048]{0,2,1,3:T(2,128)(2,1)S(1)}, u32[]{:S(2)}, u32[]{:S(2)}) %all-to-all-start.7) | async-done | bytes 1048608 | tf_op jit(solution)/shard_map/all_to_all | solution.py:140
  778.8 6.4 all-to-all-start.5
  785.2 1.5 reduce_sum.136
  786.8 1.0 copy.118
  787.8 20.0 %all-to-all-done.5 = bf16[128,8,16]{2,1,0:T(8,128)(2,1)S(1)} async-done(((bf16[128,8,16]{2,1,0:T(8,128)(2,1)}), bf16[128,8,16]{2,1,0:T(8,128)(2,1)S(1)}, u32[]{:S(2)}, u32[]{:S(2)}) %all-to-all-start.5) | async-done | bytes 32800 | tf_op jit(solution)/shard_map/all_to_all | solution.py:37
  807.8 6.2 all-to-all-start.8
  814.5 12.9 %psum.15 = bf16[8,2048]{1,0:T(8,128)(2,1)S(1)} all-reduce(bf16[8,2048]{1,0:T(8,128)(2,1)S(1)} %all_to_all.94), channel_id=1, replica_groups=mesh['ep'=128,'tp'=4] {'tp'}, use_global_device_ids=true, to_apply=%region_11.12 | all-reduce | flops 16384 | bytes 65536 | tf_op jit(solution)/shard_map/psum | solution.py:38
  827.4 9.1 %all-to-all-done.8 = bf16[128,1,2,512]{3,2,1,0:T(2,128)(2,1)S(1)} async-done(((bf16[128,1,2,512]{3,2,1,0:T(2,128)(2,1)}), bf16[128,1,2,512]{3,2,1,0:T(2,128)(2,1)S(1)}, u32[]{:S(2)}, u32[]{:S(2)}) %all-to-all-start.8) | async-done | bytes 262176 | tf_op jit(solution)/shard_map/all_to_all | solution.py:145
  (114 shorter events, 12.6 us)
Async XLA Ops:
  6.5 721.0 %copy-start = (bf16[1,176,2048]{2,1,0:T(8,128)(2,1)S(1)}, bf16[1,176,2048]{2,1,0:T(8,128)(2,1)}, u32[]{:S(2)}) copy-start(bf16[1,176,2048]{2,1,0:T(8,128)(2,1)} %param.45) | copy-start | bytes 2162692
  6.5 288.6 %reduce-scatter.3.cloned.1.call-start = ((), (), s32[]{:S(2)}) async-start(), calls=%async_computation.11 | async-start | bytes 2113536 | tf_op jit(solution)/shard_map/reduce_scatter | solution.py:21
  52.9 1.1 copy-start.1
  54.3 0.7 copy-start.12
  54.4 242.2 %copy-start.13 = (f32[64]{0:T(128)S(1)}, f32[64]{0:T(128)}, u32[]{:S(2)}) copy-start(f32[64]{0:T(128)} %param.29) | copy-start | bytes 772
  54.4 242.3 %copy-start.11 = (f32[64]{0:T(128)S(1)}, f32[64]{0:T(128)}, u32[]{:S(2)}) copy-start(f32[64]{0:T(128)} %param.28) | copy-start | bytes 772
  54.5 243.1 %copy-start.15 = (f32[2]{0:T(128)S(1)}, f32[2]{0:T(128)}, u32[]{:S(2)}) copy-start(f32[2]{0:T(128)} %param.30) | copy-start | bytes 28
  55.0 242.9 %copy-start.17 = (bf16[8,1,320,128]{3,2,1,0:T(8,128)(2,1)S(1)}, bf16[8,1,320,128]{3,2,1,0:T(8,128)(2,1)}, u32[]{:S(2)}) copy-start(bf16[8,1,320,128]{3,2,1,0:T(8,128)(2,1)} %param.32) | copy-start | bytes 1966084
  55.0 243.3 %copy-start.14 = (f32[128]{0:T(128)S(1)}, f32[128]{0:T(128)}, u32[]{:S(2)}) copy-start(f32[128]{0:T(128)} %param.34) | copy-start | bytes 1540
  297.4 27.1 %copy-start.9 = (s32[8,2]{0,1:T(2,128)S(1)}, s32[8,2]{0,1:T(2,128)}, u32[]{:S(2)}) copy-start(s32[8,2]{0,1:T(2,128)} %param.41) | copy-start | bytes 196
  297.4 60.8 %copy-start.3 = (bf16[256,16]{0,1:T(8,128)(2,1)S(1)}, bf16[256,16]{0,1:T(8,128)(2,1)}, u32[]{:S(2)}) copy-start(bf16[256,16]{0,1:T(8,128)(2,1)} %param.35) | copy-start | bytes 24580
  298.3 67.4 %copy-start.10 = (f32[8,2]{0,1:T(2,128)S(1)}, f32[8,2]{0,1:T(2,128)}, u32[]{:S(2)}) copy-start(f32[8,2]{0,1:T(2,128)} %param.42) | copy-start | bytes 196
  299.2 102.5 %copy-start.2 = (bf16[8,2048]{1,0:T(8,128)(2,1)S(1)}, bf16[8,2048]{1,0:T(8,128)(2,1)}, u32[]{:S(2)}) copy-start(bf16[8,2048]{1,0:T(8,128)(2,1)} %param.23) | copy-start | bytes 98308
  299.2 102.7 %copy-start.7 = (f32[2048]{0:T(1024)S(1)}, f32[2048]{0:T(1024)}, u32[]{:S(2)}) copy-start(f32[2048]{0:T(1024)} %param.36) | copy-start | bytes 24580
  299.2 59.0 %all-to-all-start.1 = ((bf16[128,8,256]{2,1,0:T(8,128)(2,1)}), bf16[128,8,256]{2,1,0:T(8,128)(2,1)S(1)}, u32[]{:S(2)}, u32[]{:S(2)}) async-start(bf16[128,8,256]{2,1,0:T(8,128)(2,1)} %stack.4), calls=%async_computation.2 | async-start | bytes 1048576 | tf_op jit(solution)/shard_map/all_to_all | solution.py:32
  359.3 28.8 %all-to-all-start.2 = ((bf16[128,8,16]{2,1,0:T(8,128)(2,1)}), bf16[128,8,16]{2,1,0:T(8,128)(2,1)S(1)}, u32[]{:S(2)}, u32[]{:S(2)}) async-start(bf16[128,8,16]{2,1,0:T(8,128)(2,1)} %bitcast.19), calls=%async_computation.3 | async-start | bytes 524288 | tf_op jit(solution)/shard_map/all_to_all | solution.py:37
  403.1 32.5 %all-to-all-start.3 = ((bf16[8,128,16]{2,0,1:T(8,128)(2,1)}), bf16[8,128,16]{2,0,1:T(8,128)(2,1)S(1)}, u32[]{:S(2)}, u32[]{:S(2)}) async-start(bf16[8,128,16]{2,0,1:T(8,128)(2,1)} %copy.108), calls=%async_computation.4 | async-start | bytes 524288 | tf_op jit(solution)/shard_map/all_to_all | solution.py:20
  413.4 30.2 %copy-start.4 = (bf16[16,256]{1,0:T(8,128)(2,1)S(1)}, bf16[16,256]{1,0:T(8,128)(2,1)}, u32[]{:S(2)}) copy-start(bf16[16,256]{1,0:T(8,128)(2,1)} %param.38) | copy-start | bytes 24580
  413.4 30.2 %copy-start.5 = (bf16[16,256]{1,0:T(8,128)(2,1)S(1)}, bf16[16,256]{1,0:T(8,128)(2,1)}, u32[]{:S(2)}) copy-start(bf16[16,256]{1,0:T(8,128)(2,1)} %param.37) | copy-start | bytes 24580
  437.3 262.7 %all-to-all-start.6 = ((bf16[128,2,2048]{2,1,0:T(2,128)(2,1)}), bf16[128,2,2048]{2,1,0:T(2,128)(2,1)S(1)}, u32[]{:S(2)}, u32[]{:S(2)}) async-start(bf16[128,2,2048]{2,1,0:T(2,128)(2,1)} %bitcast.26), calls=%async_computation.8 | async-start | bytes 2097152 | tf_op jit(solution)/shard_map/all_to_all | solution.py:130
  443.5 255.7 %reduce-scatter.5.cloned.1.call-start = ((), (), s32[]{:S(2)}) async-start(), calls=%async_computation.12 | async-start | bytes 2113536 | tf_op jit(solution)/shard_map/reduce_scatter | solution.py:21
  445.4 280.7 %copy-start.16 = (bf16[1,2048,176]{1,2,0:T(8,128)(2,1)S(1)}, bf16[1,2048,176]{1,2,0:T(8,128)(2,1)}, u32[]{:S(2)}) copy-start(bf16[1,2048,176]{1,2,0:T(8,128)(2,1)} %param.43) | copy-start | bytes 2162692
  700.9 58.9 %all-to-all-start.4 = ((bf16[128,8,256]{2,1,0:T(8,128)(2,1)}), bf16[128,8,256]{2,1,0:T(8,128)(2,1)S(1)}, u32[]{:S(2)}, u32[]{:S(2)}) async-start(bf16[128,8,256]{2,1,0:T(8,128)(2,1)} %stack.5), calls=%async_computation.6 | async-start | bytes 1048576 | tf_op jit(solution)/shard_map/all_to_all | solution.py:32
  732.1 31.6 %copy-start.6 = (bf16[256,16]{0,1:T(8,128)(2,1)S(1)}, bf16[256,16]{0,1:T(8,128)(2,1)}, u32[]{:S(2)}) copy-start(bf16[256,16]{0,1:T(8,128)(2,1)} %param.39) | copy-start | bytes 24580
  759.7 19.1 %all-to-all-start.7 = ((bf16[128,1,2,2048]{0,2,1,3:T(2,128)(2,1)}), bf16[128,1,2,2048]{0,2,1,3:T(2,128)(2,1)S(1)}, u32[]{:S(2)}, u32[]{:S(2)}) async-start(bf16[128,1,2,2048]{0,2,1,3:T(2,128)(2,1)} %copy.116), calls=%async_computation.9 | async-start | bytes 2097152 | tf_op jit(solution)/shard_map/all_to_all | solution.py:140
  778.8 28.9 %all-to-all-start.5 = ((bf16[128,8,16]{2,1,0:T(8,128)(2,1)}), bf16[128,8,16]{2,1,0:T(8,128)(2,1)S(1)}, u32[]{:S(2)}, u32[]{:S(2)}) async-start(bf16[128,8,16]{2,1,0:T(8,128)(2,1)} %bitcast.24), calls=%async_computation.7 | async-start | bytes 524288 | tf_op jit(solution)/shard_map/all_to_all | solution.py:37
  785.2 28.8 %copy-start.8 = (f32[2048]{0:T(1024)S(1)}, f32[2048]{0:T(1024)}, u32[]{:S(2)}) copy-start(f32[2048]{0:T(1024)} %param.40) | copy-start | bytes 24580
  807.8 28.8 %all-to-all-start.8 = ((bf16[128,1,2,512]{3,2,1,0:T(2,128)(2,1)}), bf16[128,1,2,512]{3,2,1,0:T(2,128)(2,1)S(1)}, u32[]{:S(2)}, u32[]{:S(2)}) async-start(bf16[128,1,2,512]{3,2,1,0:T(2,128)(2,1)} %copy.118), calls=%async_computation.10 | async-start | bytes 524288 | tf_op jit(solution)/shard_map/all_to_all | solution.py:145
Sparse Core Ops, SparseCore 0:
  53.0 242.0 reduce-scatter.2
  449.0 250.2 reduce-scatter.4
